TPU v7x, 256 devices: a whole 4x4x8 slice. The times are simulated.
256 devices in a mesh: sp: 32 (over z, y), tp: 8 (over x, core).
Axes of the slice: x: 4, y: 4, z: 8, core: 2. Of those that a mesh axis runs over, the one named last changes fastest.
Arguments:
- stream: bfloat16 [32768, 2048], P(('sp', 'tp')), may hold values from -6 to 6
- query_rows: bfloat16 [32768, 1024], P('sp', 'tp'), may hold values from -6 to 6
- key_rows: bfloat16 [32768, 1024], P('sp', 'tp'), may hold values from -6 to 6
- value_rows: bfloat16 [32768, 2048], P('sp', 'tp'), may hold values from -6 to 6
- gate_rows: bfloat16 [32768, 2048], P('sp', 'tp'), may hold values from -6 to 6
- log_decay: float32 [32768, 1024], P('sp', 'tp'), may hold values from -1 to 0
- head_gain: float32 [256], replicated, may hold values from 0.1 to 1.9
- out_weight: bfloat16 [2048, 2048], P('tp'), may hold values from -0.125 to 0.125
- mix_gain: float32 [2048], replicated, may hold values from 0.1 to 1.9
- up_weight: bfloat16 [2048, 8192], P('sp', 'tp'), may hold values from -0.125 to 0.125
- down_weight: bfloat16 [2048, 8192], P('sp', 'tp'), may hold values from -0.0625 to 0.0625
Outputs:
- mixed_out: bfloat16 [32768, 2048], P(('sp', 'tp'))
All inputs are finite; a program needn't handle non-finite values.
Results may differ from a plain program's by a relative error of at most 0.02.
Values may be sent and summed in bfloat16 or wider, within the bound.
A program may use at most 128 MiB of HBM per device.

v0:
```python
import jax
import jax.numpy as jnp
from jax import lax
from jax.sharding import Mesh
from jax.sharding import PartitionSpec as P

KEY_CHANNELS = 128
DV = 256
BLOCK = 64
SP = ("sp_0", "sp_1")
TP = ("tp_0", "tp_1")
SP_TP = ("sp_0", "sp_1", "tp_0", "tp_1")


EPS = 1e-06


def sent_together(arrays, axis, dim, along):
    both = jnp.concatenate(arrays, axis=along)
    result, at, outs = (lax.all_gather(both, axis, axis=dim, tiled=True), 0, [])
    for a in arrays:
        outs.append(lax.slice_in_dim(result, at, at + a.shape[along], axis=along))
        at += a.shape[along]
    return tuple(outs)


def filled_with(shard, identity):
    return jax.tree.map(
        lambda a, e: jnp.broadcast_to(jnp.asarray(e, a.dtype), a.shape), shard, identity
    )


def carried_in(shard, axes, combine, identity):
    before = start = filled_with(shard, identity)
    subtotal = shard
    for axis in reversed(axes):
        count, here = (lax.axis_size(axis), lax.axis_index(axis))
        pieces = jax.tree.map(
            lambda part, kind: lax.all_gather(part.astype(kind), axis),
            subtotal,
            (jnp.bfloat16, jnp.bfloat16),
        )
        inside, subtotal = (start, start)
        for k in range(count):
            passed = k < here
            subtotal = combine(
                subtotal, jax.tree.map(lambda part, own: part[k].astype(own.dtype), pieces, shard)
            )
            inside = jax.tree.map(lambda new, old: jnp.where(passed, new, old), subtotal, inside)
        before = combine(inside, before)
    return before


def from_everyone(shard, axis):
    copies = jnp.broadcast_to(shard, (lax.axis_size(axis), *shard.shape))
    return lax.all_to_all(copies, axis, split_axis=0, concat_axis=0, tiled=True)


def joined_along(blocks, dim):
    blocks = jnp.moveaxis(blocks, 0, dim)
    shape = blocks.shape
    return blocks.reshape(*shape[:dim], shape[dim] * shape[dim + 1], *shape[dim + 2 :])


def whole_of(shard, axes, dim):
    far, near = axes
    leading = from_everyone(shard, far)
    blocks = jnp.swapaxes(from_everyone(leading, near), 0, 1)
    return joined_along(blocks.reshape(-1, *shard.shape), dim)


def split_up(shard, dim, count):
    shape = shard.shape
    blocks = shard.reshape(*shape[:dim], count, shape[dim] // count, *shape[dim + 1 :])
    return jnp.moveaxis(blocks, dim, 0)


def summed_on_arrival(shard, axis, dim):
    blocks = split_up(shard, dim, lax.axis_size(axis))
    arrived = lax.all_to_all(blocks, axis, split_axis=0, concat_axis=0, tiled=True)
    return arrived.astype(jnp.float32).sum(axis=0)


def summed_rows(shard, axes, dim):
    far, near = axes
    own = summed_on_arrival(split_up(shard, dim, lax.axis_size(far)), near, dim + 1)
    return jnp.sum(
        lax.all_to_all(own.astype(jnp.bfloat16), far, 0, 0, tiled=True).astype(jnp.float32), axis=0
    )


def chain(earlier, later):
    return (earlier[0] * later[0], later[0][..., None] * earlier[1] + later[1])


def squared_relu(pre):
    return jnp.square(jax.nn.relu(pre)).astype(jnp.bfloat16)


def local(
    stream,
    query_rows,
    key_rows,
    value_rows,
    gate_rows,
    log_decay,
    head_gain,
    out_weight,
    mix_gain,
    up_weight,
    down_weight,
):
    up_full, down_full = sent_together((up_weight, down_weight), SP, 0, 1)
    rows = query_rows.shape[0]
    heads_here = query_rows.shape[1] // KEY_CHANNELS
    count = rows // BLOCK
    queries = query_rows.astype(jnp.float32).reshape(
        count, BLOCK, heads_here, KEY_CHANNELS
    ) * KEY_CHANNELS ** (-0.5)
    keys_all = key_rows.astype(jnp.float32).reshape(count, BLOCK, heads_here, KEY_CHANNELS)
    values_all = value_rows.astype(jnp.float32).reshape(count, BLOCK, heads_here, DV)
    decay_rates = log_decay.reshape(count, BLOCK, heads_here, KEY_CHANNELS)
    cum = jnp.cumsum(decay_rates, axis=1)
    last = cum[:, -1:]
    decayed_state = keys_all * jnp.exp(last - cum)
    state_updates = jnp.einsum(
        "nshk,nshv->nhkv", decayed_state, values_all, precision=lax.Precision.HIGHEST
    )
    end_log = last[:, 0]
    total_log = jnp.cumsum(end_log, axis=0)
    tail_weights = jnp.exp(total_log[-1] - total_log)
    summary_state = jnp.einsum(
        "mfa,mfaq->faq", tail_weights, state_updates, precision=lax.Precision.HIGHEST
    )
    summary_decay = jnp.exp(total_log[-1])
    incoming = carried_in(
        (summary_decay, summary_state),
        SP,
        chain,
        (jnp.ones_like(summary_decay), jnp.zeros_like(summary_state)),
    )

    def step(matrix_state, inputs):
        factor, state_update, query_block = inputs
        matrix_state = factor[..., None] * matrix_state + state_update
        head_output = jnp.einsum(
            "wle,leg->wlg", query_block, matrix_state, precision=lax.Precision.HIGHEST
        )
        return (matrix_state, head_output)

    _, outs = lax.scan(step, incoming[1], (jnp.exp(end_log), state_updates, queries))
    readout = outs.reshape(rows, heads_here, DV)
    scaled = readout * lax.rsqrt(jnp.mean(readout * readout, axis=-1, keepdims=True) + EPS)
    gates = gate_rows.astype(jnp.float32).reshape(rows, heads_here, DV)
    gated = scaled * head_gain * jax.nn.silu(gates)
    heads_out = gated.reshape(rows, heads_here * DV).astype(jnp.bfloat16)
    whole_weight = lax.all_gather(out_weight, TP, axis=0, tiled=True)
    mine = lax.all_to_all(heads_out, TP, split_axis=0, concat_axis=1, tiled=True)
    attn = jnp.dot(mine, whole_weight, preferred_element_type=jnp.float32)
    midf = (stream.astype(jnp.float32) + attn).astype(jnp.bfloat16).astype(jnp.float32)
    normed = (
        midf * lax.rsqrt(jnp.mean(midf * midf, axis=-1, keepdims=True) + EPS) * mix_gain
    ).astype(jnp.bfloat16)
    hidden = squared_relu(
        jnp.dot(whole_of(normed, ("tp_0", "tp_1"), 0), up_full, preferred_element_type=jnp.float32)
    )
    feed = summed_rows(
        lax.dot_general(
            hidden, down_full, (((1,), (1,)), ((), ())), preferred_element_type=jnp.float32
        ).astype(jnp.bfloat16),
        ("tp_0", "tp_1"),
        0,
    )
    return (midf + feed).astype(jnp.bfloat16)


def solution(mesh):
    torus = Mesh(mesh.devices.reshape(8, 4, 4, 2), ("sp_0", "sp_1", "tp_0", "tp_1"))
    in_specs = (
        P(SP_TP, None),
        P(SP, TP),
        P(SP, TP),
        P(SP, TP),
        P(SP, TP),
        P(SP, TP),
        P(),
        P(TP, None),
        P(),
        P(SP, TP),
        P(SP, TP),
    )
    out_specs = P(SP_TP, None)
    return jax.shard_map(local, mesh=torus, in_specs=in_specs, out_specs=out_specs, check_vma=False)
```

profile of v0, /device:TPU:1, one launch (start us, length us, event | category | flops | bytes accessed | tf_op | source)
XLA Modules:
  0.0 230.5 jit_solution(192312045876691673)
XLA Ops:
  7.3 1.7 pad_maximum_fusion
  9.0 1.4 fusion.26
  10.4 8.8 %all_gather.24 = bf16[4,1,128]{2,1,0:T(2,128)(2,1)S(1)} all-gather(bf16[1,1,128]{2,1,0:T(2,128)(2,1)S(1)} %get-tuple-element.83), channel_id=1, replica_groups=mesh['sp_0'=8,'sp_1'=4,'tp_0'=4,'tp_1'=2] {'sp_1'}, dimensions={0}, use_global_device_ids=true | all-gather | bytes 1280 | tf_op jit(solution)/shard_map/all_gather | solution.py:39
  19.3 1.0 convert.32
  20.3 16.6 %all_gather.25 = bf16[8,1,128]{2,1,0:T(2,128)(2,1)S(1)} all-gather(bf16[1,1,128]{2,1,0:T(2,128)(2,1)S(1)} %multiply_convert_fusion.2), channel_id=1, replica_groups=mesh['sp_0'=8,'sp_1'=4,'tp_0'=4,'tp_1'=2] {'sp_0'}, dimensions={0}, use_global_device_ids=true | all-gather | bytes 2304 | tf_op jit(solution)/shard_map/all_gather | solution.py:39
  37.3 1.1 fusion.24
  38.4 2.3 %fusion.14 = bf16[128,1,256]{2,1,0:T(2,128)(2,1)S(1)} fusion(f32[16,128,1]{0,2,1:T(1,128)S(1)} %copy.48, f32[16,128,256]{2,1,0:T(8,128)S(1)} %fusion.24), kind=kOutput, calls=%fused_computation.18 | convolution fusion | flops 6291456 | bytes 2170880 | tf_op jit(solution)/shard_map/mfa,mfaq->faq/dot_general | solution.py:132
  40.8 10.7 %all-gather = bf16[512,256]{1,0:T(8,128)(2,1)S(1)} all-gather(bf16[128,256]{1,0:T(8,128)(2,1)S(1)} %bitcast.258), channel_id=2, replica_groups=mesh['sp_0'=8,'sp_1'=4,'tp_0'=4,'tp_1'=2] {'sp_1'}, dimensions={0}, use_global_device_ids=true | all-gather | bytes 327680 | tf_op jit(solution)/shard_map/all_gather | solution.py:39
  51.7 20.5 %all_gather.28 = bf16[8,1,128,256]{3,2,1,0:T(8,128)(2,1)S(1)} all-gather(bf16[1,1,128,256]{3,2,1,0:T(8,128)(2,1)S(1)} %fusion.35), channel_id=1, replica_groups=mesh['sp_0'=8,'sp_1'=4,'tp_0'=4,'tp_1'=2] {'sp_0'}, dimensions={0}, use_global_device_ids=true | all-gather | bytes 589824 | tf_op jit(solution)/shard_map/all_gather | solution.py:39
  72.6 15.5 %while.12 = (s32[]{:T(128)}, f32[1,128,256]{2,1,0:T(8,128)S(1)}, f32[16,64,1,256]{3,1,2,0:T(8,128)}, f32[16,1,128]{2,1,0:T(1,128)S(1)}, f32[16,1,128,256]{3,2,1,...) while((s32[]{:T(128)}, f32[1,128,256]{2,1,0:T(8,128)S(1)}, f32[16,64,1,256]{3,1,2,0:T(8,128)}, ...), condition=%wide.region_3.4_spmd, body=%wide.region_2.3_spmd.sunk | while | flops 25231360 | bytes 690265 | solution.py:151
  73.7 0.9 fusion.84
  76.6 0.9 fusion.84
  77.6 0.8 fusion.84
  78.5 0.8 fusion.84
  79.5 0.8 fusion.84
  81.5 0.8 fusion.84
  84.4 0.9 fusion.84
  86.3 0.9 fusion.84
  88.1 1.5 multiply_reduce_fusion.1
  89.7 1.8 fusion.21
  91.5 25.3 %all_to_all.36 = bf16[8,128,256]{2,1,0:T(8,128)(2,1)S(1)} all-to-all(bf16[8,128,256]{2,1,0:T(8,128)(2,1)S(1)} %bitcast.254), channel_id=1, replica_groups=mesh['sp_0'=8,'sp_1'=4,'tp_0'=4,'tp_1'=2] {'tp_0','tp_1'}, dimensions={0} | all-to-all | bytes 1048576 | tf_op jit(solution)/shard_map/all_to_all | solution.py:158
  117.1 5.3 %multiply_reduce_fusion = (f32[128]{0:T(128)S(1)}, f32[128,2048]{1,0:T(8,128)S(1)}) fusion(bf16[128,2048]{0,1:T(8,128)(2,1)S(1)} %bitcast.251, bf16[2048,2048]{1,0:T(8,128)(2,1)} %all-gather.4.cloned.1.call-done, bf16[128,2048]{1,0:T(8,128)(2,1)S(1)} %copy-done.2), kind=kOutput, calls=%fused_computation.30 | convolution fusion | flops 1075314560 | bytes 10486272 | tf_op jit(solution)/shard_map/dot_general | solution.py:159
  122.8 27.9 %all_to_all.37 = bf16[4,128,2048]{2,1,0:T(8,128)(2,1)S(1)} all-to-all(bf16[4,128,2048]{2,1,0:T(8,128)(2,1)S(1)} %broadcast_in_dim.24), channel_id=1, replica_groups=mesh['sp_0'=8,'sp_1'=4,'tp_0'=4,'tp_1'=2] {'tp_0'}, dimensions={0} | all-to-all | bytes 4194304 | tf_op jit(solution)/shard_map/all_to_all | solution.py:56
  151.2 8.7 %all_to_all.38 = bf16[2,4,128,2048]{3,2,1,0:T(8,128)(2,1)S(1)} all-to-all(bf16[2,4,128,2048]{3,2,1,0:T(8,128)(2,1)S(1)} %broadcast_in_dim.25), channel_id=1, replica_groups=mesh['sp_0'=8,'sp_1'=4,'tp_0'=4,'tp_1'=2] {'tp_1'}, dimensions={0} | all-to-all | bytes 8388608 | tf_op jit(solution)/shard_map/all_to_all | solution.py:56
  159.9 2.3 copy.46
  162.1 3.0 %all-gather.6.cloned.1.call-done = bf16[2048,2048]{1,0:T(8,128)(2,1)} async-done(((bf16[64,2048]{1,0:T(8,128)(2,1)}), bf16[2048,2048]{1,0:T(8,128)(2,1)}) %all-gather.6.cloned.1.call-update) | async-done | bytes 8388624 | tf_op jit(solution)/shard_map/all_gather | solution.py:20
  165.2 8.1 %multiply_convert_fusion = bf16[1024,1024]{1,0:T(8,128)(2,1)S(1)} fusion(bf16[1024,2048]{1,0:T(8,128)(2,1)} %bitcast.249, bf16[2048,2048]{1,0:T(8,128)(2,1)} %all-gather.6.cloned.1.call-done), kind=kOutput, calls=%fused_computation.13 | convolution fusion | flops 4298113024 | bytes 10485760 | tf_op jit(solution)/shard_map/dot_general | solution.py:165
  173.3 4.8 %fusion.7 = bf16[1024,2048]{1,0:T(8,128)(2,1)S(1)} fusion(bf16[1024,1024]{1,0:T(8,128)(2,1)S(1)} %multiply_convert_fusion, bf16[2048,2048]{1,0:T(8,128)(2,1)S(1)} %copy-done.6), kind=kOutput, calls=%fused_computation.14 | convolution fusion | flops 4297064448 | bytes 10485760 | tf_op jit(solution)/shard_map/dot_general | solution.py:168
  178.6 9.2 %all_to_all.39 = bf16[2,4,128,2048]{3,2,1,0:T(8,128)(2,1)} all-to-all(bf16[2,4,128,2048]{3,2,1,0:T(8,128)(2,1)S(1)} %bitcast.247), channel_id=1, replica_groups=mesh['sp_0'=8,'sp_1'=4,'tp_0'=4,'tp_1'=2] {'tp_1'}, dimensions={0} | all-to-all | bytes 8388608 | tf_op jit(solution)/shard_map/all_to_all | solution.py:80
  187.8 5.1 %reduce_sum.41 = bf16[4,128,2048]{2,1,0:T(8,128)(2,1)} reduce(bf16[2,4,128,2048]{3,2,1,0:T(8,128)(2,1)} %all_to_all.39, bf16[]{:T(256)} %constant.67.clone.1), dimensions={0}, to_apply=%region_6.7 | reduce | flops 1048576 | bytes 6291458 | tf_op jit(solution)/shard_map/reduce_sum | solution.py:81
  192.9 29.4 %all_to_all.40 = bf16[4,128,2048]{2,1,0:T(8,128)(2,1)S(1)} all-to-all(bf16[4,128,2048]{2,1,0:T(8,128)(2,1)} %reduce_sum.41), channel_id=1, replica_groups=mesh['sp_0'=8,'sp_1'=4,'tp_0'=4,'tp_1'=2] {'tp_0'}, dimensions={0} | all-to-all | bytes 4194304 | tf_op jit(solution)/shard_map/all_to_all | solution.py:88
  222.7 0.9 add_convert_fusion
  (101 shorter events, 12.5 us)
Async XLA Ops:
  6.5 30.8 %copy-start = (bf16[1024,256]{1,0:T(8,128)(2,1)S(1)}, bf16[1024,256]{1,0:T(8,128)(2,1)}, u32[]{:S(2)}) copy-start(bf16[1024,256]{1,0:T(8,128)(2,1)} %param.16) | copy-start | bytes 1572868
  6.5 110.5 %all-gather.4.cloned.1.call-start = ((), (), s32[]{:S(2)}) async-start(), calls=%async_computation.5 | async-start | bytes 9437184 | tf_op jit(solution)/shard_map/all_gather | solution.py:157
  7.3 157.9 %all-gather.6.cloned.1.call-start = ((), (), s32[]{:S(2)}) async-start(), calls=%async_computation.6 | async-start | bytes 8650752 | tf_op jit(solution)/shard_map/all_gather | solution.py:20
  37.3 35.2 %copy-start.3 = (bf16[1024,128]{1,0:T(8,128)(2,1)S(1)}, bf16[1024,128]{1,0:T(8,128)(2,1)}, u32[]{:S(2)}) copy-start(bf16[1024,128]{1,0:T(8,128)(2,1)} %param.14) | copy-start | bytes 786436
  40.7 49.0 %copy-start.5 = (f32[256]{0:T(256)S(1)}, f32[256]{0:T(256)}, u32[]{:S(2)}) copy-start(f32[256]{0:T(256)} %param.19) | copy-start | bytes 3076
  88.1 28.9 %copy-start.2 = (bf16[128,2048]{1,0:T(8,128)(2,1)S(1)}, bf16[128,2048]{1,0:T(8,128)(2,1)}, u32[]{:S(2)}) copy-start(bf16[128,2048]{1,0:T(8,128)(2,1)} %param.13) | copy-start | bytes 1572868
  117.1 5.3 %copy-start.4 = (f32[2048]{0:T(1024)S(1)}, f32[2048]{0:T(1024)}, u32[]{:S(2)}) copy-start(f32[2048]{0:T(1024)} %param.21) | copy-start | bytes 24580
  165.2 8.1 %copy-start.6 = (bf16[2048,2048]{1,0:T(8,128)(2,1)S(1)}, bf16[2048,2048]{1,0:T(8,128)(2,1)}, u32[]{:S(2)}) copy-start(bf16[2048,2048]{1,0:T(8,128)(2,1)} %all-gather.6.cloned.1.call-done) | copy-start | bytes 25165828
  187.8 35.9 %copy-start.1 = (bf16[1024,256]{1,0:T(8,128)(2,1)S(1)}, bf16[1024,256]{1,0:T(8,128)(2,1)}, u32[]{:S(2)}) copy-start(bf16[1024,256]{1,0:T(8,128)(2,1)} %param.16) | copy-start | bytes 1572868
Sparse Core Ops, SparseCore 0:
  9.2 56.3 all-gather.3
  68.2 96.9 all-gather.5
where the time goes:
time: 231 us
  blocking collectives  157 us (68%)
  matrix products  35 us (15%)
  other arithmetic  16.3 us (7%)
  between operations  13.7 us (6%)
  local copies, waits for them, and re-layouts  4.33 us (2%)
  waiting for transfers between devices  3.77 us (2%)
    all_gather x4, blocking collectives, carried_in(): lax.all_gather(part.astype(kind), axis)  56.6 us
    all_to_all x2, blocking collectives, from_everyone(): return lax.all_to_all(copies, axis, split_axis=0, concat_axis=0, tiled=True)  36.5 us
    all_to_all x1, blocking collectives, summed_rows(): lax.all_to_all(own.astype(jnp.bfloat16), far, 0, 0, tiled=True)  29.4 us
    all_to_all x1, blocking collectives, local(): lax.all_to_all(heads_out, TP, split_axis=0, concat_axis=1, tiled=True)  25.3 us
    dot_general x16, matrix products, step(): jnp.einsum('wle,leg->wlg', query_block, matrix_state, precision=lax.Preci...  13.5 us
    all_to_all x1, blocking collectives, summed_on_arrival(): lax.all_to_all(blocks, axis, split_axis=0, concat_axis=0, tiled=True)  9.19 us
    dot_general x1, matrix products, local(): jnp.dot(whole_of(normed, ('tp_0', 'tp_1'), 0), up_full, preferred_element...  8.08 us
    dot_general x1, matrix products, local(): attn = jnp.dot(mine, whole_weight, preferred_element_type=jnp.float32)  5.28 us
  transfers between devices with their start and end apart: 2, of which 1 were waited for; matrix products, arithmetic and copies ran while one was open for 16% of the time, Pallas kernels for 0%

commit v1 on v0

v1 whole, which is shorter than its diff:
```python
import functools

import jax
import jax.numpy as jnp
from jax import lax
from jax.experimental import pallas as pl
from jax.experimental.pallas import tpu as pltpu
from jax.sharding import Mesh
from jax.sharding import PartitionSpec as P

KC = 128
DV = 256
BLOCK = 64
D = 2048
ROWS = 1024
OWN = 128
NB = ROWS // BLOCK
NZ, NY, NX = 8, 4, 4
NSP = NZ * NY
Q = 2
QR = OWN // Q
HID = 1024
WR = 64
EPS = 1e-06
SP = ("sp_0", "sp_1")
TP = ("tp_0", "tp_1")
SP_TP = ("sp_0", "sp_1", "tp_0", "tp_1")
MESH = pl.DeviceIdType.MESH
F32 = jnp.float32
BF16 = jnp.bfloat16

_IDS = {}


def _id(name):
    return _IDS.setdefault(name, len(_IDS))


for _d in range(2):
    _id(("ay", _d))
    _id(("ayh", _d))
    for _i in (1, 2, 3, 4):
        _id(("bz", _d, _i))
        for _h in range(2):
            _id(("az", _d, _i, _h))
    for _k in range(8):
        _id(("by", _d, _k))
        _id(("byh", _d, _k))
    for _q in range(Q):
        for _rs in range(2):
            for _j in range(4):
                _id(("dd", _rs, _j, _q))
            for _s in (1, 2):
                _id(("rx", _rs, _s, _d, _q))
        _id(("ag", _d, _q))
        _id(("agh", _d, _q))
        for _j in range(4):
            _id(("ags", _j, _q))
_id("st1")
_id("st2")
N_IDS = len(_IDS)


def _dot(a, b, dims=(((1,), (0,)), ((), ()))):
    return lax.dot_general(a, b, dims, preferred_element_type=F32)


def _split(x):
    hi = x.astype(BF16)
    return hi, (x - hi.astype(F32)).astype(BF16)


def kernel(
    stream_h,
    q_h,
    k_h,
    v_h,
    g_h,
    ld_h,
    hg_ref,
    ow_h,
    mg_ref,
    up_h,
    dn_h,
    out_ref,
    stream_v,
    q_v,
    k_v,
    v_v,
    g_v,
    ld_v,
    ow_v,
    wu,
    wd,
    sloc,
    cl,
    sx_send,
    sx_recv,
    px_send,
    px_recv,
    psend,
    precv,
    pown,
    cs,
    r1,
    r2,
    nrm,
    mid_v,
    hid_v,
    lsem,
    ssem,
    rsem,
):
    z, y = lax.axis_index("sp_0"), lax.axis_index("sp_1")
    x, c = lax.axis_index("tp_0"), lax.axis_index("tp_1")
    sp = z * NY + y
    yl, yr = lax.rem(y + NY - 1, NY), lax.rem(y + 1, NY)
    zl, zr = lax.rem(z + NZ - 1, NZ), lax.rem(z + 1, NZ)
    xl, xr = lax.rem(x + NX - 1, NX), lax.rem(x + 1, NX)
    y_to, y_from = ({"sp_1": yr}, {"sp_1": yl}), (yl, yr)
    z_to = ({"sp_0": zr}, {"sp_0": zl})
    x_to = ({"tp_0": xr}, {"tp_0": xl})
    sib = {"tp_1": 1 - c}

    barrier = pltpu.get_barrier_semaphore()

    def greet(d, carry):
        t = lax.rem(sp + d, NSP)
        pl.semaphore_signal(
            barrier, inc=1, device_id={"sp_0": t // NY, "sp_1": lax.rem(t, NY)}, device_id_type=MESH
        )
        return carry

    loads = {}

    def load(name, src, dst, i):
        loads[name] = pltpu.make_async_copy(src, dst, lsem.at[i])
        loads[name].start()

    load("ld", ld_h, ld_v, 0)
    load("k", k_h, k_v, 1)
    load("v", v_h, v_v, 2)
    load("up", up_h, wu.at[sp], 3)
    load("dn", dn_h, wd.at[sp], 4)
    load("q", q_h, q_v, 5)
    load("g", g_h, g_v, 6)
    load("ow", ow_h, ow_v, 7)
    load("stream", stream_h, stream_v, 8)

    lax.fori_loop(1, NSP, greet, 0)
    for other in (x_to[0], x_to[1], sib):
        pl.semaphore_signal(barrier, inc=1, device_id=other, device_id_type=MESH)
    pl.semaphore_wait(barrier, NSP - 1 + 3)

    copies = {}

    def send(name, src, dst, to):
        i = _IDS[name]
        copies[name] = pltpu.make_async_remote_copy(
            src_ref=src,
            dst_ref=dst,
            send_sem=ssem.at[i],
            recv_sem=rsem.at[i],
            device_id=to,
            device_id_type=MESH,
        )
        copies[name].start()

    def arrived(name):
        copies[name].wait_recv()

    HALF = (pl.ds(0, WR // 2), pl.ds(WR // 2, WR // 2))

    def zat(off):
        return lax.rem(z + off + NZ, NZ)

    def up_slab(zz, h):
        return wu.at[pl.ds(zz * NY, NY), HALF[h]]

    def up_y():
        for d in range(2):
            send(("ay", d), wu.at[sp], wu.at[sp], y_to[d])

    def up_y_half():
        for d in range(2):
            arrived(("ay", d))
            part = wu.at[z * NY + y_from[d], HALF[d]]
            send(("ayh", d), part, part, y_to[d])

    def up_z(i):
        if i == 1:
            for d in range(2):
                arrived(("ayh", d))
        for h in range(2):
            for d in range(2):
                if i > 1:
                    arrived(("az", d, i - 1, h))
                if i == 4 and h != d:
                    continue
                part = up_slab(zat(-(i - 1) if d == 0 else i - 1), h)
                send(("az", d, i, h), part, part, z_to[d])

    def up_done():
        for d in range(2):
            arrived(("az", d, 4, d))

    def dn_z(i):
        for d in range(2):
            if i > 1:
                arrived(("bz", d, i - 1))
            blk = zat(-(i - 1) if d == 0 else i - 1) * NY + y
            part = wd.at[blk] if i < 4 else wd.at[blk, HALF[d]]
            send(("bz", d, i), part, part, z_to[d])

    def dn_z_done():
        for d in range(2):
            arrived(("bz", d, 4))

    def dn_y(k):
        part = wd.at[zat(k) * NY + y]
        for d in range(2):
            send(("by", d, k), part, part, y_to[d])

    def dn_y_half(k):
        for d in range(2):
            arrived(("by", d, k))
            part = wd.at[zat(k) * NY + y_from[d], HALF[d]]
            send(("byh", d, k), part, part, y_to[d])

    def dn_done():
        for k in range(8):
            for d in range(2):
                arrived(("byh", d, k))

    loads["up"].wait()
    loads["dn"].wait()
    dn_z(1)
    up_y()
    dn_y(0)

    loads["ld"].wait()
    loads["k"].wait()
    loads["v"].wait()
    r_i = lax.broadcasted_iota(jnp.int32, (256, 256), 0)
    c_i = lax.broadcasted_iota(jnp.int32, (256, 256), 1)
    tri = jnp.where((c_i > r_i) & (c_i // BLOCK == r_i // BLOCK), 1.0, 0.0).astype(BF16)

    def group(gi, carry):
        state, total = carry
        rows = pl.ds(pl.multiple_of(gi * 256, 256), 256)
        ld = ld_v[rows, :]
        hi, lo = _split(ld)
        lo2 = (ld - hi.astype(F32) - lo.astype(F32)).astype(BF16)
        suf = _dot(tri, hi) + _dot(tri, lo) + _dot(tri, lo2)
        dk = k_v[rows, :].astype(F32) * jnp.exp(suf)
        dk_hi, dk_lo = _split(dk)
        vals = v_v[rows, :]
        for b in range(4):
            s = slice(b * BLOCK, (b + 1) * BLOCK)
            vv = jnp.concatenate([vals[s], vals[s]], axis=0)
            dd = jnp.concatenate([dk_hi[s], dk_lo[s]], axis=0)
            upd = _dot(vv, dd, (((0,), (0,)), ((), ())))
            last = suf[b * BLOCK : b * BLOCK + 1] + ld[b * BLOCK : b * BLOCK + 1]
            state = jnp.exp(last) * state + upd
            total = total + last
            sloc[gi * 4 + b] = state
            cl[gi * 4 + b] = jnp.broadcast_to(total, (8, KC))
        return state, total

    state, total = lax.fori_loop(
        0, NB // 4, group, (jnp.zeros((DV, KC), F32), jnp.zeros((1, KC), F32))
    )

    t_hi, t_lo = _split(total)
    t_lo2 = (total - t_hi.astype(F32) - t_lo.astype(F32)).astype(BF16)
    sub = lax.broadcasted_iota(jnp.int32, (8, KC), 0)
    logs = jnp.where(
        sub == 0,
        t_hi.astype(F32),
        jnp.where(sub == 1, t_lo.astype(F32), jnp.where(sub == 2, t_lo2.astype(F32), 0.0)),
    )
    tiles = jnp.concatenate(
        [state.reshape(NSP, 8, KC), jnp.broadcast_to(logs[None], (NSP, 8, KC))], axis=1
    ).astype(BF16)
    sx_send[...] = tiles

    def all_of(dst, name, sem):
        part = dst.at[pl.ds(0, NSP - 1)]
        return pltpu.make_async_copy(part, part, sem.at[_IDS[name]])

    def scatter(src, dst, name):
        i = _IDS[name]

        def one(d, carry):
            t = lax.rem(sp + d, NSP)
            pltpu.make_async_remote_copy(
                src_ref=src.at[t],
                dst_ref=dst.at[sp],
                send_sem=ssem.at[i],
                recv_sem=rsem.at[i],
                device_id={"sp_0": t // NY, "sp_1": lax.rem(t, NY)},
                device_id_type=MESH,
            ).start()
            return carry

        lax.fori_loop(1, NSP, one, 0)
        dst[sp] = src[sp]

    scatter(sx_send, sx_recv, "st1")

    up_y_half()
    dn_z(2)
    dn_y(1)
    dn_y(7)

    all_of(sx_recv, "st1", rsem).wait()

    def prefix(e, run):
        px_send[e] = run
        tile = sx_recv[e].astype(F32)
        log = tile[8:9] + tile[9:10] + tile[10:11]
        return jnp.exp(log) * run + tile[0:8]

    lax.fori_loop(0, NSP, prefix, jnp.zeros((8, KC), F32))
    scatter(px_send, px_recv, "st2")

    dn_y_half(0)
    up_z(1)
    dn_z(3)
    dn_y(2)
    dn_y(6)

    loads["q"].wait()
    loads["g"].wait()
    loads["ow"].wait()
    all_of(px_recv, "st2", rsem).wait()

    def attend(j):
        s_in = px_recv[...].reshape(DV, KC)
        base = lax.rem(x + j, NX) * 4
        gain = hg_ref[...]
        outs = []
        for half in range(2):
            first = base + (1 - c if half == 0 else c) * 2
            for b in range(2):
                n = first + b
                rows = pl.ds(pl.multiple_of(n * BLOCK, BLOCK), BLOCK)
                full = sloc[n] + jnp.exp(cl[n][0:1]) * s_in
                f_hi, f_lo = _split(full)
                qq = q_v[rows, :]
                read = _dot(
                    jnp.concatenate([qq, qq], axis=1),
                    jnp.concatenate([f_hi, f_lo], axis=1),
                    (((1,), (1,)), ((), ())),
                ) * (KC**-0.5)
                scaled = read * lax.rsqrt(jnp.mean(read * read, axis=-1, keepdims=True) + EPS)
                gate = g_v[rows, :].astype(F32)
                outs.append((scaled * gain * (gate / (1.0 + jnp.exp(-gate)))).astype(BF16))
        heads = jnp.concatenate(outs, axis=0)
        for n in range(4):
            cols = slice(n * 512, (n + 1) * 512)
            part = _dot(heads, ow_v[:, cols])
            for q in range(Q):
                psend[0, j, q, :, cols] = part[q * QR : (q + 1) * QR].astype(BF16)
                pown[j, q, :, cols] = part[OWN + q * QR : OWN + (q + 1) * QR]
        for q in range(Q):
            pair_send(0, j, q)

    def pair_send(rs, j, q):
        send(("dd", rs, j, q), psend.at[rs, j, q], precv.at[rs, j, q], sib)

    def pair_sum(rs, j, q):
        arrived(("dd", rs, j, q))
        return pown[j, q] + precv[rs, j, q].astype(F32)

    H2 = QR // 2

    def ring_1(rs, q):
        cs[rs, 0, q] = pair_sum(rs, 2, q).astype(BF16)
        for d in range(2):
            send(
                ("rx", rs, 1, d, q), cs.at[rs, 0, q, pl.ds(d * H2, H2)], r1.at[rs, d, q], x_to[d]
            )

    def ring_2(rs, q):
        for d in range(2):
            j = 1 if d == 0 else 3
            both = pair_sum(rs, j, q)
            arrived(("rx", rs, 1, d, q))
            more = r1[rs, d, q].astype(F32)
            if d == 0:
                both = jnp.concatenate([both[:H2] + more, both[H2:]], axis=0)
            else:
                both = jnp.concatenate([both[:H2], both[H2:] + more], axis=0)
            cs[rs, 1 + d, q] = both.astype(BF16)
            send(("rx", rs, 2, d, q), cs.at[rs, 1 + d, q], r2.at[rs, d, q], x_to[d])

    def ring_end(rs, q):
        total = pair_sum(rs, 0, q)
        for d in range(2):
            arrived(("rx", rs, 2, d, q))
            total = total + r2[rs, d, q].astype(F32)
        return total

    attend(2)
    attend(1)
    for q in range(Q):
        ring_1(0, q)
    dn_y_half(1)
    dn_y_half(7)
    dn_z(4)
    up_z(2)
    dn_y(3)
    dn_y(5)
    attend(3)
    attend(0)
    for q in range(Q):
        ring_2(0, q)

    loads["stream"].wait()

    def spread_rows(q):
        mid = (stream_v[pl.ds(q * QR, QR), :].astype(F32) + ring_end(0, q)).astype(BF16)
        mid_v[q] = mid
        midf = mid.astype(F32)
        nrm[1, 0, q] = (
            midf * lax.rsqrt(jnp.mean(midf * midf, axis=-1, keepdims=True) + EPS) * mg_ref[...]
        ).astype(BF16)
        for d in range(2):
            send(("ag", d, q), nrm.at[1, 0, q], nrm.at[1, 3 if d == 0 else 1, q], x_to[d])
        send(("ags", 0, q), nrm.at[1, 0, q], nrm.at[0, 0, q], sib)

    def spread_mid(q):
        for d in range(2):
            arrived(("ag", d, q))
            j = 3 if d == 0 else 1
            rows = pl.ds(d * H2, H2)
            send(("agh", d, q), nrm.at[1, j, q, rows], nrm.at[1, 2, q, rows], x_to[d])
            send(("ags", j, q), nrm.at[1, j, q], nrm.at[0, j, q], sib)

    def spread_end(q):
        for d in range(2):
            arrived(("agh", d, q))
        send(("ags", 2, q), nrm.at[1, 2, q], nrm.at[0, 2, q], sib)

    def spread_done(q):
        for j in range(4):
            arrived(("ags", j, q))

    def ff_up(q):
        def tile(n, carry):
            cols = pl.ds(pl.multiple_of(n * 256, 256), 256)
            pre = _dot(nrm[:, :, q].reshape(8 * QR, D), wu[:, :, cols].reshape(D, 256))
            pre = jnp.maximum(pre, 0.0)
            hid_v[:, cols] = (pre * pre).astype(BF16)
            return carry

        lax.fori_loop(0, HID // 256, tile, 0)

    def ff_down(q):
        def tile(n, carry):
            cols = pl.ds(pl.multiple_of(n * 256, 256), 256)
            part = _dot(
                hid_v[...], wd[pl.ds(n * 4, 4)].reshape(256, HID), (((1,), (1,)), ((), ()))
            ).reshape(2, 4, QR, 256)
            psend[1, :, q, :, cols] = part[0].astype(BF16)
            pown[:, q, :, cols] = part[1]
            return carry

        lax.fori_loop(0, D // 256, tile, 0)
        for j in (2, 1, 3, 0):
            pair_send(1, j, q)

    dn_z_done()
    dn_y(4)
    dn_y_half(2)
    dn_y_half(6)
    up_z(3)
    spread_rows(0)
    spread_rows(1)
    dn_y_half(3)
    dn_y_half(5)
    up_z(4)
    spread_mid(0)
    spread_mid(1)
    dn_y_half(4)
    spread_end(0)
    up_done()
    spread_done(0)
    ff_up(0)
    spread_end(1)
    dn_done()
    ff_down(0)
    ring_1(1, 0)
    spread_done(1)
    ff_up(1)
    ring_2(1, 0)
    ff_down(1)
    ring_1(1, 1)
    ring_2(1, 1)
    for q in range(Q):
        out_ref[pl.ds(q * QR, QR), :] = (mid_v[q].astype(F32) + ring_end(1, q)).astype(BF16)

    for name in copies:
        copies[name].wait_send()
    all_of(sx_send, "st1", ssem).wait()
    all_of(px_send, "st2", ssem).wait()


def local(
    stream,
    query_rows,
    key_rows,
    value_rows,
    gate_rows,
    log_decay,
    head_gain,
    out_weight,
    mix_gain,
    up_weight,
    down_weight,
):
    any_spec = pl.BlockSpec(memory_space=pl.ANY)
    vmem = pl.BlockSpec(memory_space=pltpu.VMEM)
    return pl.pallas_call(
        kernel,
        out_shape=jax.ShapeDtypeStruct((OWN, D), BF16),
        in_specs=[any_spec] * 6 + [vmem, any_spec, vmem, any_spec, any_spec],
        out_specs=vmem,
        scratch_shapes=[
            pltpu.VMEM((OWN, D), BF16),
            pltpu.VMEM((ROWS, KC), BF16),
            pltpu.VMEM((ROWS, KC), BF16),
            pltpu.VMEM((ROWS, DV), BF16),
            pltpu.VMEM((ROWS, DV), BF16),
            pltpu.VMEM((ROWS, KC), F32),
            pltpu.VMEM((DV, D), BF16),
            pltpu.VMEM((NSP, WR, HID), BF16),
            pltpu.VMEM((NSP, WR, HID), BF16),
            pltpu.VMEM((NB, DV, KC), F32),
            pltpu.VMEM((NB, 8, KC), F32),
            pltpu.VMEM((NSP, 16, KC), BF16),
            pltpu.VMEM((NSP, 16, KC), BF16),
            pltpu.VMEM((NSP, 8, KC), F32),
            pltpu.VMEM((NSP, 8, KC), F32),
            pltpu.VMEM((2, 4, Q, QR, D), BF16),
            pltpu.VMEM((2, 4, Q, QR, D), BF16),
            pltpu.VMEM((4, Q, QR, D), F32),
            pltpu.VMEM((2, 3, Q, QR, D), BF16),
            pltpu.VMEM((2, 2, Q, QR // 2, D), BF16),
            pltpu.VMEM((2, 2, Q, QR, D), BF16),
            pltpu.VMEM((2, 4, Q, QR, D), BF16),
            pltpu.VMEM((Q, QR, D), BF16),
            pltpu.VMEM((8 * QR, HID), BF16),
            pltpu.SemaphoreType.DMA((10,)),
            pltpu.SemaphoreType.DMA((N_IDS,)),
            pltpu.SemaphoreType.DMA((N_IDS,)),
        ],
        compiler_params=pltpu.CompilerParams(
            collective_id=0, has_side_effects=True, vmem_limit_bytes=60 * 1024 * 1024
        ),
        name="layer",
    )(
        stream,
        query_rows,
        key_rows,
        value_rows,
        gate_rows,
        log_decay,
        head_gain.reshape(1, DV),
        out_weight,
        mix_gain.reshape(1, D),
        up_weight,
        down_weight,
    )


def solution(mesh):
    torus = Mesh(mesh.devices.reshape(NZ, NY, NX, 2), SP_TP)
    in_specs = (
        P(SP_TP, None),
        P(SP, TP),
        P(SP, TP),
        P(SP, TP),
        P(SP, TP),
        P(SP, TP),
        P(),
        P(TP, None),
        P(),
        P(SP, TP),
        P(SP, TP),
    )
    out_specs = P(SP_TP, None)
    return jax.shard_map(local, mesh=torus, in_specs=in_specs, out_specs=out_specs, check_vma=False)
```

time: 231 us -> 107 us (0.46)
  blocking collectives: 157 us -> 0 us
  Pallas kernels: 0 us -> 105 us
  matrix products: 35 us -> 0 us
  other arithmetic: 16.3 us -> 0 us
  between operations: 13.7 us -> 0.01 us
  waiting for transfers between devices: 3.77 us -> 0 us
  local copies, waits for them, and re-layouts: 4.33 us -> 1.88 us
    pallas_call x0 -> x1, Pallas kernels: none -> 105 us  [local(): pl.pallas_call(kernel, out_shape=jax.ShapeDtypeStruct((OWN, D), BF16), in...]
    all_to_all x5 -> x0, blocking collectives: 100 us -> none  [the longest x2 36.5 us: from_everyone(): return lax.all_to_all(copies, axis, split_axis=0, concat_axis=0, tiled=True)]
    all_gather x4 -> x0, blocking collectives: 56.6 us -> none  [carried_in(): lax.all_gather(part.astype(kind), axis)]
    dot_general x21 -> x0, matrix products: 35 us -> none  [the longest x16 13.5 us: step(): jnp.einsum('wle,leg->wlg', query_block, matrix_state, precision=lax.Preci...]
    reduce_sum x3 -> x0, other arithmetic: 6.95 us -> none  [the longest x1 5.08 us: summed_on_arrival(): return arrived.astype(jnp.float32).sum(axis=0)]
    all_gather x2 -> x0, waiting for transfers between devices: 3.04 us -> none  [the longest x1 3.02 us: sent_together(): result, at, outs = (lax.all_gather(both, axis, axis=dim, tiled=True), 0, [])]
    convert_element_type x7 -> x0, other arithmetic: 3.01 us -> none  [the longest x1 1.76 us: local(): heads_out = gated.reshape(rows, heads_here * DV).astype(jnp.bfloat16)]
    all_to_all x2 -> x0, local copies, waits for them, and re-layouts: 2.53 us -> none  [the longest x1 2.26 us: from_everyone(): return lax.all_to_all(copies, axis, split_axis=0, concat_axis=0, tiled=True)]
  transfers between devices with their start and end apart: 2 -> 0, of which waited for: 1 -> 0; matrix products, arithmetic and copies ran while one was open for 16% -> 0% of each run, Pallas kernels for 0% -> 0%
where the time goes in v1:
time: 107 us; the launch traced here: 106 us
  Pallas kernels  105 us (98%)
  local copies, waits for them, and re-layouts  1.88 us (2%)
    pallas_call x1, Pallas kernels, local(): pl.pallas_call(kernel, out_shape=jax.ShapeDtypeStruct((OWN, D), BF16), in...  105 us

profile of v1, /device:TPU:1, one launch (start us, length us, event | category | flops | bytes accessed | tf_op | source)
XLA Modules:
  0.0 106.4 jit_solution(15155169766841032634)
XLA Ops:
  0.0 104.5 %layer.1 = bf16[128,2048]{1,0:T(8,128)(2,1)} custom-call(bf16[128,2048]{1,0:T(8,128)(2,1)} %stream_h.1, bf16[1024,128]{1,0:T(8,128)(2,1)} %q_h.1, bf16[1024,128]{1,0:T(8,128)(2,1)} %k_h.1, bf16[1024,256]{1,0:T(8,128)(2,1)} %v_h.1, bf16[1024,256]{1,0:T(8,128)(2,1)} %g_h.1, f32[1024,128]{1,0:T(8,128)} %ld_h.1, f32[1,256]{1,0:T(1,128)} %bitcast.3, ...), custom_call_target="tpu_custom_call" | custom-call | tf_op jit(solution)/shard_map/layer/pallas_call | solution.py:525
  104.6 1.9 %copy.13 = bf16[128,2048]{1,0:T(8,128)(2,1)} copy(bf16[128,2048]{1,0:T(8,128)(2,1)} %layer.1) | data formatting | bytes 1048576

commit v2 on v1

v2 whole, which is shorter than its diff:
```python
import functools

import jax
import jax.numpy as jnp
from jax import lax
from jax.experimental import pallas as pl
from jax.experimental.pallas import tpu as pltpu
from jax.sharding import Mesh
from jax.sharding import PartitionSpec as P

KC = 128
DV = 256
BLOCK = 64
D = 2048
ROWS = 1024
OWN = 128
NB = ROWS // BLOCK
NZ, NY, NX = 8, 4, 4
NSP = NZ * NY
Q = 4
QR = OWN // Q
FR = OWN // 2
HID = 1024
WR = 64
AC = 768
EPS = 1e-06
SP = ("sp_0", "sp_1")
TP = ("tp_0", "tp_1")
SP_TP = ("sp_0", "sp_1", "tp_0", "tp_1")
MESH = pl.DeviceIdType.MESH
F32 = jnp.float32
BF16 = jnp.bfloat16

G = 4
CH1 = tuple((q * QR, QR, 0, D) for q in range(Q))
CH2 = tuple((f * FR, FR, g * (D // G), D // G) for f in range(2) for g in range(G))
CHUNKS = (CH1, CH2)
SLOT = {2: 0, 1: 1, 3: 2, 0: 3}

RECV, SEND = {}, {}


def _recv_id(*name):
    RECV.setdefault(name, len(RECV))
    SEND.setdefault(name[0], len(SEND))


for _n in ("ay", "ayh", "st1", "st2", "st3"):
    _recv_id(_n)
for _i in (1, 2, 3, 4):
    _recv_id("bz", _i)
    for _h in range(2 if _i < 4 else 1):
        _recv_id("az", _i, _h)
for _k in range(8):
    _recv_id("by", _k)
    _recv_id("byh", _k)
for _n in ((2, 0), (2, 1), 1, 3, 0):
    _recv_id("dd0", _n)
for _n in range(len(CH2)):
    _recv_id("dd1", 0, _n)
    _recv_id("dd1", 1, _n)
for _rs in range(2):
    for _n in range(len(CHUNKS[_rs])):
        for _s in (1, 2):
            _recv_id(("rx", _rs, _s), _n)
for _q in range(Q):
    _recv_id("ag", _q)
    _recv_id("agh", _q)
for _f in range(2):
    _recv_id("ags", _f)


def _dot(a, b, dims=(((1,), (0,)), ((), ()))):
    return lax.dot_general(a, b, dims, preferred_element_type=F32)


def _split(x):
    hi = x.astype(BF16)
    return hi, (x - hi.astype(F32)).astype(BF16)


def kernel(
    stream_h,
    q_h,
    k_h,
    v_h,
    g_h,
    ld_h,
    hg_h,
    ow_h,
    mg_h,
    up_h,
    dn_h,
    out_ref,
    hg_ref,
    mg_ref,
    stream_v,
    q_v,
    k_v,
    v_v,
    g_v,
    ld_v,
    ow_v,
    w,
    wt,
    sloc,
    cl,
    sx_send,
    sx_recv,
    zx_send,
    zx_recv,
    px_send,
    px_recv,
    psend,
    precv,
    pown,
    cs,
    r1,
    r2,
    nrm,
    mid_v,
    hid_v,
    lsem,
    ssem,
    rsem,
):
    z, y = lax.axis_index("sp_0"), lax.axis_index("sp_1")
    x, c = lax.axis_index("tp_0"), lax.axis_index("tp_1")
    sp = z * NY + y
    yl, yr = lax.rem(y + NY - 1, NY), lax.rem(y + 1, NY)
    zl, zr = lax.rem(z + NZ - 1, NZ), lax.rem(z + 1, NZ)
    xl, xr = lax.rem(x + NX - 1, NX), lax.rem(x + 1, NX)
    y_to, y_from = ({"sp_1": yr}, {"sp_1": yl}), (yl, yr)
    z_to = ({"sp_0": zr}, {"sp_0": zl})
    x_to = ({"tp_0": xr}, {"tp_0": xl})
    sib = {"tp_1": 1 - c}

    barrier = pltpu.get_barrier_semaphore()

    def signal_to(other):
        pl.semaphore_signal(barrier, inc=1, device_id=other, device_id_type=MESH)

    def greet_y(d, carry):
        signal_to({"sp_1": lax.rem(y + d, NY)})
        return carry

    def greet_z(d, carry):
        signal_to({"sp_0": lax.rem(z + d, NZ)})
        return carry

    lax.fori_loop(1, NY, greet_y, 0)
    lax.fori_loop(1, NZ, greet_z, 0)
    for other in (x_to[0], x_to[1], sib):
        signal_to(other)

    loads = {}

    def load(name, src, dst, i):
        loads[name] = pltpu.make_async_copy(src, dst, lsem.at[i])
        loads[name].start()

    load("ld", ld_h, ld_v, 0)
    load("k", k_h, k_v, 1)
    load("v", v_h, v_v, 2)
    load("up", up_h, w.at[sp, :, pl.ds(0, HID)], 3)
    load("dn", dn_h, w.at[sp, :, pl.ds(HID, HID)], 4)
    load("q", q_h, q_v, 5)
    load("g", g_h, g_v, 6)
    load("ow", ow_h, ow_v, 7)
    load("stream", stream_h, stream_v, 8)
    load("hg", hg_h, hg_ref, 9)
    load("mg", mg_h, mg_ref, 10)

    def send(name, src, dst, to):
        pltpu.make_async_remote_copy(
            src_ref=src,
            dst_ref=dst,
            send_sem=ssem.at[SEND[name[0]]],
            recv_sem=rsem.at[RECV[name]],
            device_id=to,
            device_id_type=MESH,
        ).start()

    waited = set()

    def arrived(name, size):
        if name not in waited:
            waited.add(name)
            pltpu.make_async_copy(size, size, rsem.at[RECV[name]]).wait()

    def sent(family, size):
        pltpu.make_async_copy(size, size, ssem.at[SEND[family]]).wait()

    HALF = (pl.ds(0, WR // 2), pl.ds(WR // 2, WR // 2))
    COLS_A, COLS_B = pl.ds(0, AC), pl.ds(AC, 2 * HID - AC)

    def zat(off):
        return lax.rem(z + off + NZ, NZ)

    def some_a(n):
        return w.at[pl.ds(0, n), :, COLS_A]

    def some_b(n):
        return w.at[pl.ds(0, n), :, COLS_B]

    def up_y():
        for d in range(2):
            part = w.at[sp, :, COLS_A]
            send(("ay",), part, part, y_to[d])

    def up_y_half():
        arrived(("ay",), some_a(2))
        for d in range(2):
            part = w.at[z * NY + y_from[d], HALF[d], COLS_A]
            send(("ayh",), part, part, y_to[d])

    def up_z(i, step):
        if i == 1:
            arrived(("ayh",), some_a(1))
        else:
            arrived(("az", i - 1, step), some_a(4))
        if i < 4 or step == 0:
            for d in range(2):
                zz = zat(-(i - 1) if d == 0 else i - 1)
                part = w.at[pl.ds(zz * NY, NY), HALF[step if d == 0 else 1 - step], COLS_A]
                send(("az", i, step), part, part, z_to[d])

    def up_done():
        arrived(("az", 4, 0), some_a(4))

    def dn_z(i):
        if i > 1:
            arrived(("bz", i - 1), some_b(2))
        for d in range(2):
            blk = zat(-(i - 1) if d == 0 else i - 1) * NY + y
            part = w.at[blk, :, COLS_B] if i < 4 else w.at[blk, HALF[d], COLS_B]
            send(("bz", i), part, part, z_to[d])

    def dn_y(k):
        if k in (1, 7):
            arrived(("bz", 1), some_b(2))
        if k == 4:
            arrived(("bz", 4), some_b(1))
        part = w.at[zat(k) * NY + y, :, COLS_B]
        for d in range(2):
            send(("by", k), part, part, y_to[d])

    def dn_y_half(k):
        arrived(("by", k), some_b(2))
        for d in range(2):
            part = w.at[zat(k) * NY + y_from[d], HALF[d], COLS_B]
            send(("byh", k), part, part, y_to[d])

    def dn_turn(k):
        arrived(("byh", k), some_b(1))
        zz = zat(k)
        slab = w[pl.ds(zz * NY, NY), :, pl.ds(HID, HID)].reshape(NY * WR, HID)
        wt[:, pl.ds(pl.multiple_of(zz * NY * WR, NY * WR), NY * WR)] = slab.T

    loads["ld"].wait()
    loads["k"].wait()
    loads["v"].wait()
    r_i = lax.broadcasted_iota(jnp.int32, (256, 256), 0)
    c_i = lax.broadcasted_iota(jnp.int32, (256, 256), 1)
    tri = jnp.where((c_i > r_i) & (c_i // BLOCK == r_i // BLOCK), 1.0, 0.0).astype(BF16)

    def group(gi, carry):
        state, total = carry
        rows = pl.ds(pl.multiple_of(gi * 256, 256), 256)
        ld = ld_v[rows, :]
        hi, lo = _split(ld)
        lo2 = (ld - hi.astype(F32) - lo.astype(F32)).astype(BF16)
        suf = _dot(tri, hi) + _dot(tri, lo) + _dot(tri, lo2)
        dk = k_v[rows, :].astype(F32) * jnp.exp(suf)
        dk_hi, dk_lo = _split(dk)
        vals = v_v[rows, :]
        for b in range(4):
            s = slice(b * BLOCK, (b + 1) * BLOCK)
            vv = jnp.concatenate([vals[s], vals[s]], axis=0)
            dd = jnp.concatenate([dk_hi[s], dk_lo[s]], axis=0)
            upd = _dot(vv, dd, (((0,), (0,)), ((), ())))
            last = suf[b * BLOCK : b * BLOCK + 1] + ld[b * BLOCK : b * BLOCK + 1]
            state = jnp.exp(last) * state + upd
            total = total + last
            sloc[gi * 4 + b] = state
            cl[gi * 4 + b] = jnp.broadcast_to(total, (8, KC))
        return state, total

    state, total = lax.fori_loop(
        0, NB // 4, group, (jnp.zeros((DV, KC), F32), jnp.zeros((1, KC), F32))
    )

    QV = DV // NY

    def with_log(block, log):
        hi, lo = _split(log)
        lo2 = (log - hi.astype(F32) - lo.astype(F32)).astype(BF16)
        sub = lax.broadcasted_iota(jnp.int32, (16, KC), 0)
        logs = jnp.where(
            sub == 0,
            hi.astype(F32),
            jnp.where(sub == 1, lo.astype(F32), jnp.where(sub == 2, lo2.astype(F32), 0.0)),
        )
        return jnp.concatenate([block, logs], axis=0).astype(BF16)

    def block_log(tile):
        t = tile.astype(F32)
        return t[:QV], t[QV : QV + 1] + t[QV + 1 : QV + 2] + t[QV + 2 : QV + 3]

    def first(ref, count):
        return ref.at[pl.ds(0, count)]

    def scatter(name, count, src_of, dst, to):
        def one(d, carry):
            pltpu.make_async_remote_copy(
                src_ref=src_of(d),
                dst_ref=dst,
                send_sem=ssem.at[SEND[name]],
                recv_sem=rsem.at[RECV[(name,)]],
                device_id=to(d),
                device_id_type=MESH,
            ).start()
            return carry

        lax.fori_loop(1, count, one, 0)

    def y_at(d):
        return lax.rem(y + d, NY)

    for p in range(NY):
        sx_send[p] = with_log(state[p * QV : (p + 1) * QV], total)

    pl.semaphore_wait(barrier, NY - 1 + NZ - 1 + 3)
    scatter("st1", NY, lambda d: sx_send.at[y_at(d)], sx_recv.at[y], lambda d: {"sp_1": y_at(d)})
    sx_recv[y] = sx_send[y]
    loads["up"].wait()
    loads["dn"].wait()
    up_y()
    dn_y(0)
    dn_z(1)
    arrived(("st1",), first(sx_recv, NY - 1))

    group_state, group_log = block_log(sx_recv[0])
    for p in range(1, NY):
        more, log = block_log(sx_recv[p])
        group_state = jnp.exp(log) * group_state + more
        group_log = group_log + log
    zx_send[...] = with_log(group_state, group_log)
    scatter(
        "st2", NZ, lambda d: zx_send, zx_recv.at[z], lambda d: {"sp_0": lax.rem(z + d, NZ)}
    )
    zx_recv[z] = zx_send[...]
    up_y_half()
    dn_y(1)
    arrived(("st2",), first(zx_recv, NZ - 1))

    run = jnp.zeros((QV, KC), F32)
    for e in range(NZ):
        more, log = block_log(zx_recv[e])
        run = jnp.where(e < z, jnp.exp(log) * run + more, run)
    for p in range(NY):
        px_send[p] = run.astype(BF16)
        more, log = block_log(sx_recv[p])
        run = jnp.exp(log) * run + more
    scatter("st3", NY, lambda d: px_send.at[y_at(d)], px_recv.at[y], lambda d: {"sp_1": y_at(d)})
    px_recv[y] = px_send[y]

    dn_z(2)
    dn_y(7)
    dn_y_half(0)
    up_z(1, 0)
    loads["q"].wait()
    loads["g"].wait()
    loads["ow"].wait()
    loads["hg"].wait()
    arrived(("st3",), first(px_recv, NY - 1))

    def attend(j):
        s_in = px_recv[...].astype(F32).reshape(DV, KC)
        base = lax.rem(x + j, NX) * 4
        gain = hg_ref[...]
        outs = []
        for half in range(2):
            first = base + (1 - c if half == 0 else c) * 2
            for b in range(2):
                n = first + b
                rows = pl.ds(pl.multiple_of(n * BLOCK, BLOCK), BLOCK)
                full = sloc[n] + jnp.exp(cl[n][0:1]) * s_in
                f_hi, f_lo = _split(full)
                qq = q_v[rows, :]
                read = _dot(
                    jnp.concatenate([qq, qq], axis=1),
                    jnp.concatenate([f_hi, f_lo], axis=1),
                    (((1,), (1,)), ((), ())),
                ) * (KC**-0.5)
                scaled = read * lax.rsqrt(jnp.mean(read * read, axis=-1, keepdims=True) + EPS)
                gate = g_v[rows, :].astype(F32)
                outs.append((scaled * gain * (gate / (1.0 + jnp.exp(-gate)))).astype(BF16))
        heads = jnp.concatenate(outs, axis=0)
        for n in range(4):
            cols = slice(n * 512, (n + 1) * 512)
            part = _dot(heads, ow_v[:, cols])
            psend[0, SLOT[j], :, cols] = part[:OWN].astype(BF16)
            pown[SLOT[j], :, cols] = part[OWN:]
        for name, rows in pair_parts(j):
            send(("dd0", name), psend.at[0, SLOT[j], rows], precv.at[0, SLOT[j], rows], sib)

    def views(rs, n):
        r0, nr, c0, nc = CHUNKS[rs][n]
        return pl.ds(r0, nr), pl.ds(c0, nc), pl.ds(r0 // 2, nr // 2), nr // 2, r0

    def pair_parts(j):
        if j == 2:
            return (((2, 0), pl.ds(0, QR)), ((2, 1), pl.ds(QR, OWN - QR)))
        return ((j, pl.ds(0, OWN)),)

    def pair_sum(rs, j, n):
        rows, cols, _, _, _ = views(rs, n)
        if rs == 0:
            name, part = pair_parts(j)[1 if j == 2 and n > 0 else 0]
            arrived(("dd0", name), precv.at[0, SLOT[j], part])
        elif j == 2:
            arrived(("dd1", 0, n), precv.at[1, 0, rows, cols])
        else:
            arrived(("dd1", 1, n), precv.at[1, pl.ds(1, 3), rows, cols])
        return pown[SLOT[j], rows, cols] + precv[rs, SLOT[j], rows, cols].astype(F32)

    def ring_1(rs, n):
        rows, cols, half, h2, r0 = views(rs, n)
        cs[rs, 0, rows, cols] = pair_sum(rs, 2, n).astype(BF16)
        for d in range(2):
            send(
                (("rx", rs, 1), n),
                cs.at[rs, 0, pl.ds(r0 + d * h2, h2), cols],
                r1.at[rs, d, half, cols],
                x_to[d],
            )

    def ring_2(rs, n):
        rows, cols, half, h2, _ = views(rs, n)
        both = [pair_sum(rs, 1, n), pair_sum(rs, 3, n)]
        arrived((("rx", rs, 1), n), r1.at[rs, :, half, cols])
        for d in range(2):
            more = r1[rs, d, half, cols].astype(F32)
            if d == 0:
                total = jnp.concatenate([both[d][:h2] + more, both[d][h2:]], axis=0)
            else:
                total = jnp.concatenate([both[d][:h2], both[d][h2:] + more], axis=0)
            cs[rs, 1 + d, rows, cols] = total.astype(BF16)
            send((("rx", rs, 2), n), cs.at[rs, 1 + d, rows, cols], r2.at[rs, d, rows, cols], x_to[d])

    def ring_end(rs, n):
        rows, cols, _, _, _ = views(rs, n)
        total = pair_sum(rs, 0, n)
        arrived((("rx", rs, 2), n), r2.at[rs, :, rows, cols])
        return total + r2[rs, 0, rows, cols].astype(F32) + r2[rs, 1, rows, cols].astype(F32)

    def rows_of(q):
        return pl.ds(q * QR, QR)

    def norm_rows(q):
        rows = rows_of(q)
        mid = (stream_v[rows, :].astype(F32) + ring_end(0, q)).astype(BF16)
        mid_v[rows, :] = mid
        midf = mid.astype(F32)
        nrm[1, 0, rows, :] = (
            midf * lax.rsqrt(jnp.mean(midf * midf, axis=-1, keepdims=True) + EPS) * mg_ref[...]
        ).astype(BF16)

    def spread_rows(q):
        rows = rows_of(q)
        for d in range(2):
            send(("ag", q), nrm.at[1, 0, rows], nrm.at[1, 3 if d == 0 else 1, rows], x_to[d])
        send(("ags", q // 2), nrm.at[1, 0, rows], nrm.at[0, 0, rows], sib)

    def spread_mid(q):
        rows = rows_of(q)
        arrived(("ag", q), nrm.at[1, pl.ds(0, 2), rows])
        for d in range(2):
            j = 3 if d == 0 else 1
            part = pl.ds(q * QR + d * (QR // 2), QR // 2)
            send(("agh", q), nrm.at[1, j, part], nrm.at[1, 2, part], x_to[d])
            send(("ags", q // 2), nrm.at[1, j, rows], nrm.at[0, j, rows], sib)

    def spread_end(q):
        rows = rows_of(q)
        arrived(("agh", q), nrm.at[1, 2, rows])
        send(("ags", q // 2), nrm.at[1, 2, rows], nrm.at[0, 2, rows], sib)

    def spread_done(f):
        arrived(("ags", f), nrm.at[0, :, pl.ds(f * FR, FR)])

    def ff_up(f, n):
        x_in = nrm[:, :, pl.ds(f * FR, FR)].reshape(8 * FR, D)
        for c0 in (n * 512, n * 512 + 256):
            pre = _dot(x_in, w[:, :, c0 : c0 + 256].reshape(D, 256))
            pre = jnp.maximum(pre, 0.0)
            hid_v[:, c0 : c0 + 256] = (pre * pre).astype(BF16)

    def ff_down(f, g):
        rows = slice(f * FR, (f + 1) * FR)
        for c0 in range(g * (D // G), (g + 1) * (D // G), 256):
            part = _dot(hid_v[...], wt[:, c0 : c0 + 256]).reshape(2, 4, FR, 256)
            for j in range(4):
                psend[1, SLOT[j], rows, c0 : c0 + 256] = part[0, j].astype(BF16)
                pown[SLOT[j], rows, c0 : c0 + 256] = part[1, j]
        n = G * f + g
        rows, cols, _, _, _ = views(1, n)
        for i, slots in enumerate((pl.ds(0, 1), pl.ds(1, 3))):
            send(("dd1", i, n), psend.at[1, slots, rows, cols], precv.at[1, slots, rows, cols], sib)

    def out_rows(n):
        rows, cols, _, _, _ = views(1, n)
        out_ref[rows, cols] = (mid_v[rows, cols].astype(F32) + ring_end(1, n)).astype(BF16)

    attend(2)
    attend(1)
    dn_z(3)
    dn_y(2)
    dn_y(6)
    up_z(1, 1)
    ring_1(0, 0)
    ring_1(0, 1)
    ring_1(0, 2)
    ring_1(0, 3)
    attend(3)
    attend(0)
    dn_y_half(1)
    dn_y_half(7)
    up_z(2, 0)
    ring_2(0, 0)
    ring_2(0, 1)
    ring_2(0, 2)
    dn_z(4)
    dn_y(3)
    dn_y(5)
    ring_2(0, 3)
    dn_y_half(2)
    dn_y_half(6)
    up_z(2, 1)
    loads["stream"].wait()
    loads["mg"].wait()
    norm_rows(0)
    spread_rows(0)
    dn_turn(0)
    norm_rows(1)
    spread_rows(1)
    up_z(3, 0)
    dn_y(4)
    norm_rows(2)
    dn_turn(1)
    dn_turn(7)
    up_z(3, 1)
    norm_rows(3)
    spread_mid(0)
    up_z(4, 0)
    dn_y_half(3)
    dn_y_half(5)
    spread_mid(1)
    spread_rows(2)
    spread_rows(3)
    dn_turn(2)
    dn_turn(6)
    spread_end(0)
    dn_y_half(4)
    spread_end(1)
    up_z(4, 1)
    dn_turn(3)
    dn_turn(5)
    up_done()
    spread_done(0)
    dn_turn(4)
    ff_up(0, 0)
    spread_mid(2)
    ff_up(0, 1)
    spread_mid(3)
    ff_down(0, 0)
    ff_down(0, 1)
    ff_down(0, 2)
    ring_1(1, 0)
    ff_down(0, 3)
    ring_1(1, 1)
    spread_end(2)
    spread_end(3)
    ring_1(1, 2)
    ring_1(1, 3)
    spread_done(1)
    ff_up(1, 0)
    ring_2(1, 0)
    ring_2(1, 1)
    ff_up(1, 1)
    ring_2(1, 2)
    ff_down(1, 0)
    ring_2(1, 3)
    ff_down(1, 1)
    ring_1(1, 4)
    ff_down(1, 2)
    ring_1(1, 5)
    ff_down(1, 3)
    ring_1(1, 6)
    out_rows(0)
    ring_1(1, 7)
    ring_2(1, 4)
    ring_2(1, 5)
    out_rows(1)
    out_rows(2)
    ring_2(1, 6)
    out_rows(3)
    ring_2(1, 7)
    out_rows(4)
    out_rows(5)
    out_rows(6)
    out_rows(7)

    for family, size in (
        ("ay", some_a(2)),
        ("ayh", some_a(1)),
        ("az", some_a(28)),
        ("bz", some_b(7)),
        ("by", some_b(16)),
        ("byh", some_b(8)),
        ("st1", first(sx_send, NY - 1)),
        ("st2", first(zx_recv, NZ - 1)),
        ("st3", first(px_send, NY - 1)),
        ("dd0", psend.at[0]),
        ("dd1", psend.at[1]),
        (("rx", 0, 1), cs.at[0, 0]),
        (("rx", 0, 2), cs.at[0, pl.ds(1, 2)]),
        (("rx", 1, 1), cs.at[1, 0]),
        (("rx", 1, 2), cs.at[1, pl.ds(1, 2)]),
        ("ag", nrm.at[1, pl.ds(0, 2)]),
        ("agh", nrm.at[1, 0]),
        ("ags", nrm.at[0]),
    ):
        sent(family, size)


def local(
    stream,
    query_rows,
    key_rows,
    value_rows,
    gate_rows,
    log_decay,
    head_gain,
    out_weight,
    mix_gain,
    up_weight,
    down_weight,
):
    any_spec = pl.BlockSpec(memory_space=pl.ANY)
    vmem = pl.BlockSpec(memory_space=pltpu.VMEM)
    return pl.pallas_call(
        kernel,
        out_shape=pltpu.VMEM((OWN, D), BF16),
        in_specs=[any_spec] * 11,
        out_specs=vmem,
        scratch_shapes=[
            pltpu.VMEM((1, DV), F32),
            pltpu.VMEM((1, D), F32),
            pltpu.VMEM((OWN, D), BF16),
            pltpu.VMEM((ROWS, KC), BF16),
            pltpu.VMEM((ROWS, KC), BF16),
            pltpu.VMEM((ROWS, DV), BF16),
            pltpu.VMEM((ROWS, DV), BF16),
            pltpu.VMEM((ROWS, KC), F32),
            pltpu.VMEM((DV, D), BF16),
            pltpu.VMEM((NSP, WR, 2 * HID), BF16),
            pltpu.VMEM((HID, D), BF16),
            pltpu.VMEM((NB, DV, KC), F32),
            pltpu.VMEM((NB, 8, KC), F32),
            pltpu.VMEM((NY, DV // NY + 16, KC), BF16),
            pltpu.VMEM((NY, DV // NY + 16, KC), BF16),
            pltpu.VMEM((DV // NY + 16, KC), BF16),
            pltpu.VMEM((NZ, DV // NY + 16, KC), BF16),
            pltpu.VMEM((NY, DV // NY, KC), BF16),
            pltpu.VMEM((NY, DV // NY, KC), BF16),
            pltpu.VMEM((2, 4, OWN, D), BF16),
            pltpu.VMEM((2, 4, OWN, D), BF16),
            pltpu.VMEM((4, OWN, D), F32),
            pltpu.VMEM((2, 3, OWN, D), BF16),
            pltpu.VMEM((2, 2, OWN // 2, D), BF16),
            pltpu.VMEM((2, 2, OWN, D), BF16),
            pltpu.VMEM((2, 4, OWN, D), BF16),
            pltpu.VMEM((OWN, D), BF16),
            pltpu.VMEM((8 * FR, HID), BF16),
            pltpu.SemaphoreType.DMA((11,)),
            pltpu.SemaphoreType.DMA((len(SEND),)),
            pltpu.SemaphoreType.DMA((len(RECV),)),
        ],
        compiler_params=pltpu.CompilerParams(
            collective_id=0, has_side_effects=True, vmem_limit_bytes=60 * 1024 * 1024
        ),
        name="layer",
    )(
        stream,
        query_rows,
        key_rows,
        value_rows,
        gate_rows,
        log_decay,
        head_gain.reshape(1, DV),
        out_weight,
        mix_gain.reshape(1, D),
        up_weight,
        down_weight,
    )


def solution(mesh):
    torus = Mesh(mesh.devices.reshape(NZ, NY, NX, 2), SP_TP)
    in_specs = (
        P(SP_TP, None),
        P(SP, TP),
        P(SP, TP),
        P(SP, TP),
        P(SP, TP),
        P(SP, TP),
        P(),
        P(TP, None),
        P(),
        P(SP, TP),
        P(SP, TP),
    )
    out_specs = P(SP_TP, None)
    return jax.shard_map(local, mesh=torus, in_specs=in_specs, out_specs=out_specs, check_vma=False)
```

time: 107 us -> 87.1 us (0.81)
  Pallas kernels: 105 us -> 86.2 us
  local copies, waits for them, and re-layouts: 1.88 us -> 0.8 us
    pallas_call x1, Pallas kernels: 105 us -> 86.2 us  [local(): pl.pallas_call(kernel, out_shape=pltpu.VMEM((OWN, D), BF16), in_specs=[an...]
    unnamed x1, local copies, waits for them, and re-layouts: 1.88 us -> 0.8 us
where the time goes in v2:
time: 87.1 us; the launch traced here: 87 us
  Pallas kernels  86.2 us (99%)
    pallas_call x1, Pallas kernels, local(): pl.pallas_call(kernel, out_shape=pltpu.VMEM((OWN, D), BF16), in_specs=[an...  86.2 us

profile of v2, /device:TPU:1, one launch (start us, length us, event | category | flops | bytes accessed | tf_op | source)
XLA Modules:
  0.0 87.0 jit_solution(13537356996238637307)
XLA Ops:
  0.0 86.2 %layer.1 = bf16[128,2048]{1,0:T(8,128)(2,1)S(1)} custom-call(bf16[128,2048]{1,0:T(8,128)(2,1)} %stream_h.1, bf16[1024,128]{1,0:T(8,128)(2,1)} %q_h.1, bf16[1024,128]{1,0:T(8,128)(2,1)} %k_h.1, bf16[1024,256]{1,0:T(8,128)(2,1)} %v_h.1, bf16[1024,256]{1,0:T(8,128)(2,1)} %g_h.1, f32[1024,128]{1,0:T(8,128)} %ld_h.1, f32[1,256]{1,0:T(1,128)} %bitcast.3, ...), custom_call_target="tpu_custom_call" | custom-call | tf_op jit(solution)/shard_map/layer/pallas_call | solution.py:653
  86.2 0.8 copy.13

commit v3 on v2

--- a/solution.py
+++ b/solution.py
@@ -19,7 +19,6 @@
 NSP = NZ * NY
 Q = 4
 QR = OWN // Q
-FR = OWN // 2
 HID = 1024
 WR = 64
 AC = 768
@@ -31,9 +30,9 @@
 F32 = jnp.float32
 BF16 = jnp.bfloat16
 
-G = 4
+G = 2
 CH1 = tuple((q * QR, QR, 0, D) for q in range(Q))
-CH2 = tuple((f * FR, FR, g * (D // G), D // G) for f in range(2) for g in range(G))
+CH2 = tuple((q * QR, QR, g * (D // G), D // G) for q in range(Q) for g in range(G))
 CHUNKS = (CH1, CH2)
 SLOT = {2: 0, 1: 1, 3: 2, 0: 3}
 
@@ -66,8 +65,7 @@
 for _q in range(Q):
     _recv_id("ag", _q)
     _recv_id("agh", _q)
-for _f in range(2):
-    _recv_id("ags", _f)
+    _recv_id("ags", _q)
 
 
 def _dot(a, b, dims=(((1,), (0,)), ((), ()))):
@@ -99,6 +97,7 @@
     k_v,
     v_v,
     g_v,
+    gate_v,
     ld_v,
     ow_v,
     w,
@@ -162,14 +161,6 @@
     load("ld", ld_h, ld_v, 0)
     load("k", k_h, k_v, 1)
     load("v", v_h, v_v, 2)
-    load("up", up_h, w.at[sp, :, pl.ds(0, HID)], 3)
-    load("dn", dn_h, w.at[sp, :, pl.ds(HID, HID)], 4)
-    load("q", q_h, q_v, 5)
-    load("g", g_h, g_v, 6)
-    load("ow", ow_h, ow_v, 7)
-    load("stream", stream_h, stream_v, 8)
-    load("hg", hg_h, hg_ref, 9)
-    load("mg", mg_h, mg_ref, 10)
 
     def send(name, src, dst, to):
         pltpu.make_async_remote_copy(
@@ -260,13 +251,20 @@
     loads["ld"].wait()
     loads["k"].wait()
     loads["v"].wait()
+    load("up", up_h, w.at[sp, :, pl.ds(0, HID)], 3)
+    load("dn", dn_h, w.at[sp, :, pl.ds(HID, HID)], 4)
+    load("q", q_h, q_v, 5)
+    load("g", g_h, g_v, 6)
+    load("ow", ow_h, ow_v, 7)
+    load("stream", stream_h, stream_v, 8)
+    load("hg", hg_h, hg_ref, 9)
+    load("mg", mg_h, mg_ref, 10)
     r_i = lax.broadcasted_iota(jnp.int32, (256, 256), 0)
     c_i = lax.broadcasted_iota(jnp.int32, (256, 256), 1)
     tri = jnp.where((c_i > r_i) & (c_i // BLOCK == r_i // BLOCK), 1.0, 0.0).astype(BF16)
 
-    def group(gi, carry):
-        state, total = carry
-        rows = pl.ds(pl.multiple_of(gi * 256, 256), 256)
+    def group(gi, state, total):
+        rows = slice(gi * 256, (gi + 1) * 256)
         ld = ld_v[rows, :]
         hi, lo = _split(ld)
         lo2 = (ld - hi.astype(F32) - lo.astype(F32)).astype(BF16)
@@ -286,9 +284,9 @@
             cl[gi * 4 + b] = jnp.broadcast_to(total, (8, KC))
         return state, total
 
-    state, total = lax.fori_loop(
-        0, NB // 4, group, (jnp.zeros((DV, KC), F32), jnp.zeros((1, KC), F32))
-    )
+    state, total = jnp.zeros((DV, KC), F32), jnp.zeros((1, KC), F32)
+    for gi in range(NB // 4):
+        state, total = group(gi, state, total)
 
     QV = DV // NY
 
@@ -352,6 +350,7 @@
     zx_recv[z] = zx_send[...]
     up_y_half()
     dn_y(1)
+    dn_z(2)
     arrived(("st2",), first(zx_recv, NZ - 1))
 
     run = jnp.zeros((QV, KC), F32)
@@ -365,7 +364,6 @@
     scatter("st3", NY, lambda d: px_send.at[y_at(d)], px_recv.at[y], lambda d: {"sp_1": y_at(d)})
     px_recv[y] = px_send[y]
 
-    dn_z(2)
     dn_y(7)
     dn_y_half(0)
     up_z(1, 0)
@@ -373,12 +371,19 @@
     loads["g"].wait()
     loads["ow"].wait()
     loads["hg"].wait()
+
+    def gate_rows_of(n, carry):
+        rows = pl.ds(pl.multiple_of(n * 256, 256), 256)
+        gate = g_v[rows, :].astype(F32)
+        gate_v[rows, :] = hg_ref[...] * (gate / (1.0 + jnp.exp(-gate)))
+        return carry
+
+    lax.fori_loop(0, ROWS // 256, gate_rows_of, 0)
     arrived(("st3",), first(px_recv, NY - 1))
 
     def attend(j):
         s_in = px_recv[...].astype(F32).reshape(DV, KC)
         base = lax.rem(x + j, NX) * 4
-        gain = hg_ref[...]
         outs = []
         for half in range(2):
             first = base + (1 - c if half == 0 else c) * 2
@@ -394,8 +399,7 @@
                     (((1,), (1,)), ((), ())),
                 ) * (KC**-0.5)
                 scaled = read * lax.rsqrt(jnp.mean(read * read, axis=-1, keepdims=True) + EPS)
-                gate = g_v[rows, :].astype(F32)
-                outs.append((scaled * gain * (gate / (1.0 + jnp.exp(-gate)))).astype(BF16))
+                outs.append((scaled * gate_v[rows, :]).astype(BF16))
         heads = jnp.concatenate(outs, axis=0)
         for n in range(4):
             cols = slice(n * 512, (n + 1) * 512)
@@ -471,7 +475,7 @@
         rows = rows_of(q)
         for d in range(2):
             send(("ag", q), nrm.at[1, 0, rows], nrm.at[1, 3 if d == 0 else 1, rows], x_to[d])
-        send(("ags", q // 2), nrm.at[1, 0, rows], nrm.at[0, 0, rows], sib)
+        send(("ags", q), nrm.at[1, 0, rows], nrm.at[0, 0, rows], sib)
 
     def spread_mid(q):
         rows = rows_of(q)
@@ -480,32 +484,31 @@
             j = 3 if d == 0 else 1
             part = pl.ds(q * QR + d * (QR // 2), QR // 2)
             send(("agh", q), nrm.at[1, j, part], nrm.at[1, 2, part], x_to[d])
-            send(("ags", q // 2), nrm.at[1, j, rows], nrm.at[0, j, rows], sib)
+            send(("ags", q), nrm.at[1, j, rows], nrm.at[0, j, rows], sib)
 
     def spread_end(q):
         rows = rows_of(q)
         arrived(("agh", q), nrm.at[1, 2, rows])
-        send(("ags", q // 2), nrm.at[1, 2, rows], nrm.at[0, 2, rows], sib)
-
-    def spread_done(f):
-        arrived(("ags", f), nrm.at[0, :, pl.ds(f * FR, FR)])
-
-    def ff_up(f, n):
-        x_in = nrm[:, :, pl.ds(f * FR, FR)].reshape(8 * FR, D)
-        for c0 in (n * 512, n * 512 + 256):
+        send(("ags", q), nrm.at[1, 2, rows], nrm.at[0, 2, rows], sib)
+
+    def spread_done(q):
+        arrived(("ags", q), nrm.at[0, :, rows_of(q)])
+
+    def ff_up(q, half):
+        x_in = nrm[:, :, rows_of(q)].reshape(8 * QR, D)
+        for c0 in range(half * (HID // 2), (half + 1) * (HID // 2), 256):
             pre = _dot(x_in, w[:, :, c0 : c0 + 256].reshape(D, 256))
             pre = jnp.maximum(pre, 0.0)
             hid_v[:, c0 : c0 + 256] = (pre * pre).astype(BF16)
 
-    def ff_down(f, g):
-        rows = slice(f * FR, (f + 1) * FR)
+    def ff_down(q, g):
+        n = G * q + g
+        rows, cols, _, _, _ = views(1, n)
         for c0 in range(g * (D // G), (g + 1) * (D // G), 256):
-            part = _dot(hid_v[...], wt[:, c0 : c0 + 256]).reshape(2, 4, FR, 256)
+            part = _dot(hid_v[...], wt[:, c0 : c0 + 256]).reshape(2, 4, QR, 256)
             for j in range(4):
                 psend[1, SLOT[j], rows, c0 : c0 + 256] = part[0, j].astype(BF16)
                 pown[SLOT[j], rows, c0 : c0 + 256] = part[1, j]
-        n = G * f + g
-        rows, cols, _, _, _ = views(1, n)
         for i, slots in enumerate((pl.ds(0, 1), pl.ds(1, 3))):
             send(("dd1", i, n), psend.at[1, slots, rows, cols], precv.at[1, slots, rows, cols], sib)
 
@@ -553,60 +556,66 @@
     up_z(3, 1)
     norm_rows(3)
     spread_mid(0)
+    spread_rows(2)
     up_z(4, 0)
     dn_y_half(3)
     dn_y_half(5)
     spread_mid(1)
-    spread_rows(2)
     spread_rows(3)
     dn_turn(2)
     dn_turn(6)
     spread_end(0)
     dn_y_half(4)
-    spread_end(1)
     up_z(4, 1)
+    spread_mid(2)
     dn_turn(3)
     dn_turn(5)
     up_done()
     spread_done(0)
+    ff_up(0, 0)
+    spread_end(1)
     dn_turn(4)
-    ff_up(0, 0)
-    spread_mid(2)
     ff_up(0, 1)
-    spread_mid(3)
     ff_down(0, 0)
     ff_down(0, 1)
-    ff_down(0, 2)
+    spread_done(1)
+    ff_up(1, 0)
+    spread_mid(3)
     ring_1(1, 0)
-    ff_down(0, 3)
+    ff_up(1, 1)
     ring_1(1, 1)
     spread_end(2)
+    ff_down(1, 0)
+    ff_down(1, 1)
+    spread_done(2)
+    ff_up(2, 0)
+    ring_1(1, 2)
     spread_end(3)
-    ring_1(1, 2)
+    ff_up(2, 1)
     ring_1(1, 3)
-    spread_done(1)
-    ff_up(1, 0)
     ring_2(1, 0)
+    ff_down(2, 0)
     ring_2(1, 1)
-    ff_up(1, 1)
+    ff_down(2, 1)
+    spread_done(3)
+    ff_up(3, 0)
+    ring_1(1, 4)
     ring_2(1, 2)
-    ff_down(1, 0)
+    ff_up(3, 1)
+    ring_1(1, 5)
+    ff_down(3, 0)
     ring_2(1, 3)
-    ff_down(1, 1)
-    ring_1(1, 4)
-    ff_down(1, 2)
-    ring_1(1, 5)
-    ff_down(1, 3)
+    ff_down(3, 1)
+    ring_2(1, 4)
     ring_1(1, 6)
+    ring_1(1, 7)
+    ring_2(1, 5)
     out_rows(0)
-    ring_1(1, 7)
-    ring_2(1, 4)
-    ring_2(1, 5)
+    ring_2(1, 6)
+    ring_2(1, 7)
     out_rows(1)
     out_rows(2)
-    ring_2(1, 6)
     out_rows(3)
-    ring_2(1, 7)
     out_rows(4)
     out_rows(5)
     out_rows(6)
@@ -663,6 +672,7 @@
             pltpu.VMEM((ROWS, KC), BF16),
             pltpu.VMEM((ROWS, DV), BF16),
             pltpu.VMEM((ROWS, DV), BF16),
+            pltpu.VMEM((ROWS, DV), F32),
             pltpu.VMEM((ROWS, KC), F32),
             pltpu.VMEM((DV, D), BF16),
             pltpu.VMEM((NSP, WR, 2 * HID), BF16),
@@ -683,7 +693,7 @@
             pltpu.VMEM((2, 2, OWN, D), BF16),
             pltpu.VMEM((2, 4, OWN, D), BF16),
             pltpu.VMEM((OWN, D), BF16),
-            pltpu.VMEM((8 * FR, HID), BF16),
+            pltpu.VMEM((8 * QR, HID), BF16),
             pltpu.SemaphoreType.DMA((11,)),
             pltpu.SemaphoreType.DMA((len(SEND),)),
             pltpu.SemaphoreType.DMA((len(RECV),)),

time: 87.1 us -> 84 us (0.964)
  Pallas kernels: 86.2 us -> 82.9 us
    pallas_call x1, Pallas kernels: 86.2 us -> 82.9 us  [local(): pl.pallas_call(kernel, out_shape=pltpu.VMEM((OWN, D), BF16), in_specs=[an...]
where the time goes in v3:
time: 84 us; the launch traced here: 83.7 us
  Pallas kernels  82.9 us (99%)
    pallas_call x1, Pallas kernels, local(): pl.pallas_call(kernel, out_shape=pltpu.VMEM((OWN, D), BF16), in_specs=[an...  82.9 us

profile of v3, /device:TPU:1, one launch (start us, length us, event | category | flops | bytes accessed | tf_op | source)
XLA Modules:
  0.0 83.7 jit_solution(11287039059297298086)
XLA Ops:
  0.0 82.9 %layer.1 = bf16[128,2048]{1,0:T(8,128)(2,1)S(1)} custom-call(bf16[128,2048]{1,0:T(8,128)(2,1)} %stream_h.1, bf16[1024,128]{1,0:T(8,128)(2,1)} %q_h.1, bf16[1024,128]{1,0:T(8,128)(2,1)} %k_h.1, bf16[1024,256]{1,0:T(8,128)(2,1)} %v_h.1, bf16[1024,256]{1,0:T(8,128)(2,1)} %g_h.1, f32[1024,128]{1,0:T(8,128)} %ld_h.1, f32[1,256]{1,0:T(1,128)} %bitcast.3, ...), custom_call_target="tpu_custom_call" | custom-call | tf_op jit(solution)/shard_map/layer/pallas_call | solution.py:662
  82.9 0.8 copy.13

commit v4 on v3

--- a/solution.py
+++ b/solution.py
@@ -379,6 +379,10 @@
         return carry
 
     lax.fori_loop(0, ROWS // 256, gate_rows_of, 0)
+    dn_z(3)
+    dn_y(2)
+    dn_y(6)
+    up_z(1, 1)
     arrived(("st3",), first(px_recv, NY - 1))
 
     def attend(j):
@@ -518,10 +522,6 @@
 
     attend(2)
     attend(1)
-    dn_z(3)
-    dn_y(2)
-    dn_y(6)
-    up_z(1, 1)
     ring_1(0, 0)
     ring_1(0, 1)
     ring_1(0, 2)
@@ -568,11 +568,11 @@
     dn_y_half(4)
     up_z(4, 1)
     spread_mid(2)
-    dn_turn(3)
-    dn_turn(5)
     up_done()
     spread_done(0)
     ff_up(0, 0)
+    dn_turn(3)
+    dn_turn(5)
     spread_end(1)
     dn_turn(4)
     ff_up(0, 1)
@@ -590,13 +590,13 @@
     spread_done(2)
     ff_up(2, 0)
     ring_1(1, 2)
-    spread_end(3)
     ff_up(2, 1)
     ring_1(1, 3)
+    spread_end(3)
     ring_2(1, 0)
     ff_down(2, 0)
+    ff_down(2, 1)
     ring_2(1, 1)
-    ff_down(2, 1)
     spread_done(3)
     ff_up(3, 0)
     ring_1(1, 4)

time: 84 us -> 83.8 us (level)
  no operation moved by 1% of the time
where the time goes in v4:
time: 83.8 us; the launch traced here: 83.7 us
  Pallas kernels  82.9 us (99%)
    pallas_call x1, Pallas kernels, local(): pl.pallas_call(kernel, out_shape=pltpu.VMEM((OWN, D), BF16), in_specs=[an...  82.9 us

profile of v4, /device:TPU:1, one launch (start us, length us, event | category | flops | bytes accessed | tf_op | source)
XLA Modules:
  0.0 83.7 jit_solution(835946034176746530)
XLA Ops:
  0.0 82.9 %layer.1 = bf16[128,2048]{1,0:T(8,128)(2,1)S(1)} custom-call(bf16[128,2048]{1,0:T(8,128)(2,1)} %stream_h.1, bf16[1024,128]{1,0:T(8,128)(2,1)} %q_h.1, bf16[1024,128]{1,0:T(8,128)(2,1)} %k_h.1, bf16[1024,256]{1,0:T(8,128)(2,1)} %v_h.1, bf16[1024,256]{1,0:T(8,128)(2,1)} %g_h.1, f32[1024,128]{1,0:T(8,128)} %ld_h.1, f32[1,256]{1,0:T(1,128)} %bitcast.3, ...), custom_call_target="tpu_custom_call" | custom-call | tf_op jit(solution)/shard_map/layer/pallas_call | solution.py:662
  82.9 0.8 copy.13

commit v5 on v4

--- a/solution.py
+++ b/solution.py
@@ -37,11 +37,16 @@
 SLOT = {2: 0, 1: 1, 3: 2, 0: 3}
 
 RECV, SEND = {}, {}
+FAMILY = {"ay": "az", "ayh": "az", "by": "bz", "byh": "bz", "dd1": "dd0"}
+
+
+def _family(first):
+    return "rx" if isinstance(first, tuple) else FAMILY.get(first, first)
 
 
 def _recv_id(*name):
     RECV.setdefault(name, len(RECV))
-    SEND.setdefault(name[0], len(SEND))
+    SEND.setdefault(_family(name[0]), len(SEND))
 
 
 for _n in ("ay", "ayh", "st1", "st2", "st3"):
@@ -166,7 +171,7 @@
         pltpu.make_async_remote_copy(
             src_ref=src,
             dst_ref=dst,
-            send_sem=ssem.at[SEND[name[0]]],
+            send_sem=ssem.at[SEND[_family(name[0])]],
             recv_sem=rsem.at[RECV[name]],
             device_id=to,
             device_id_type=MESH,
@@ -622,21 +627,13 @@
     out_rows(7)
 
     for family, size in (
-        ("ay", some_a(2)),
-        ("ayh", some_a(1)),
-        ("az", some_a(28)),
-        ("bz", some_b(7)),
-        ("by", some_b(16)),
-        ("byh", some_b(8)),
+        ("az", some_a(31)),
+        ("bz", some_b(31)),
         ("st1", first(sx_send, NY - 1)),
         ("st2", first(zx_recv, NZ - 1)),
         ("st3", first(px_send, NY - 1)),
-        ("dd0", psend.at[0]),
-        ("dd1", psend.at[1]),
-        (("rx", 0, 1), cs.at[0, 0]),
-        (("rx", 0, 2), cs.at[0, pl.ds(1, 2)]),
-        (("rx", 1, 1), cs.at[1, 0]),
-        (("rx", 1, 2), cs.at[1, pl.ds(1, 2)]),
+        ("dd0", psend),
+        ("rx", cs),
         ("ag", nrm.at[1, pl.ds(0, 2)]),
         ("agh", nrm.at[1, 0]),
         ("ags", nrm.at[0]),

time: 83.8 us -> 83.7 us (level)
  no operation moved by 1% of the time
where the time goes in v5:
time: 83.7 us; the launch traced here: 83.6 us
  Pallas kernels  82.8 us (99%)
    pallas_call x1, Pallas kernels, local(): pl.pallas_call(kernel, out_shape=pltpu.VMEM((OWN, D), BF16), in_specs=[an...  82.8 us

profile of v5, /device:TPU:1, one launch (start us, length us, event | category | flops | bytes accessed | tf_op | source)
XLA Modules:
  0.0 83.6 jit_solution(13750325499694327094)
XLA Ops:
  0.0 82.8 %layer.1 = bf16[128,2048]{1,0:T(8,128)(2,1)S(1)} custom-call(bf16[128,2048]{1,0:T(8,128)(2,1)} %stream_h.1, bf16[1024,128]{1,0:T(8,128)(2,1)} %q_h.1, bf16[1024,128]{1,0:T(8,128)(2,1)} %k_h.1, bf16[1024,256]{1,0:T(8,128)(2,1)} %v_h.1, bf16[1024,256]{1,0:T(8,128)(2,1)} %g_h.1, f32[1024,128]{1,0:T(8,128)} %ld_h.1, f32[1,256]{1,0:T(1,128)} %bitcast.3, ...), custom_call_target="tpu_custom_call" | custom-call | tf_op jit(solution)/shard_map/layer/pallas_call | solution.py:659
  82.8 0.8 copy.13
